TPU v7x, 32 devices: a whole 2x2x4 slice. The times are simulated.
32 devices in a mesh: ep: 4 (over y, x), tp: 8 (over z, core).
Axes of the slice: x: 2, y: 2, z: 4, core: 2. Of those that a mesh axis runs over, the one named last changes fastest.
Arguments:
- tokens: bfloat16 [2048, 2048], P('ep', 'tp'), may hold values from -6 to 6
- norm_gain: float32 [2048], replicated, may hold values from 0.1 to 1.9
- norm_shift: float32 [2048], replicated, may hold values from -3 to 3
- expert_ids: int32 [2048, 6], P('ep'), may hold values from 0 to 31, all different within a row; in each aligned block of 64 rows (0 to 63, 64 to 127, ...) at most 24 rows name the same one
- affinity: float32 [2048, 6], P('ep'), may hold values from 0.05 to 1
- expert_gate: bfloat16 [32, 2048, 512], P(('ep', 'tp')), may hold values from -0.125 to 0.125
- expert_up: bfloat16 [32, 2048, 512], P(('ep', 'tp')), may hold values from -0.125 to 0.125
- expert_down: bfloat16 [32, 512, 2048], P(('ep', 'tp')), may hold values from -0.25 to 0.25
- shared_gate: bfloat16 [512, 2048], P('tp'), may hold values from -0.125 to 0.125
- shared_up: bfloat16 [512, 2048], P('tp'), may hold values from -0.125 to 0.125
- shared_down: bfloat16 [512, 2048], replicated, may hold values from -0.25 to 0.25
Outputs:
- mixed: bfloat16 [2048, 2048], P(('ep', 'tp'))
Inputs may be any that keep to these rules, and one draw needn't show every extreme that they name: `expert_ids`: each row names 6 different experts; in each aligned block of 64 rows (the rows of one device of tp) no expert is named more than 24 times, and in some blocks an expert is named exactly 24 times.
All inputs are finite; a program needn't handle non-finite values.
Results may differ from a plain program's by a relative error of at most 0.0069.
Values may be sent and summed in bfloat16 or wider, within the bound.
A program may use at most 64 MiB of HBM per device.

v0:
```python
import jax
import jax.numpy as jnp
from jax import lax
from jax.sharding import PartitionSpec as P

ROUTED_SCALE = 2.5
EPSILON = 1e-05


def pair_ranks(flat_ids, expert_count):
    onehot = flat_ids[..., None] == jnp.arange(expert_count, dtype=jnp.int32)
    running = jnp.cumsum(onehot.astype(jnp.int32), axis=-2)
    return jnp.sum(jnp.where(onehot, running, 0), axis=-1) - 1


def expert_rows(tok_rows, w_gate, w_up, w_down):
    gate_act = jnp.dot(tok_rows, w_gate, preferred_element_type=jnp.float32)
    up_act = jnp.dot(tok_rows, w_up, preferred_element_type=jnp.float32)
    hidden = (jax.nn.silu(gate_act) * up_act).astype(jnp.bfloat16)
    return jnp.dot(hidden, w_down, preferred_element_type=jnp.float32).astype(jnp.bfloat16)


def weighted_sum(source_rows, slot_index, pair_weight, top_count):
    total = jnp.zeros((slot_index.shape[0], source_rows.shape[1]), jnp.float32)
    for column in range(top_count):
        picked = jnp.take(source_rows, slot_index[:, column], axis=0, mode="fill", fill_value=0)
        total = total + pair_weight[:, column : column + 1] * picked.astype(jnp.float32)
    return total


def on_device(
    tokens,
    norm_gain,
    norm_shift,
    expert_ids,
    affinity,
    expert_gate,
    expert_up,
    expert_down,
    shared_gate,
    shared_up,
    shared_down,
):
    ep_count = lax.axis_size("ep")
    tp_count = lax.axis_size("tp")
    tp_index = lax.axis_index("tp")
    whole = lax.all_gather(tokens, "tp", axis=1, tiled=True)
    tok_count = whole.shape[0]
    width = whole.shape[1]
    top_count = expert_ids.shape[1]
    block_rows = tok_count // tp_count
    expert_count = ep_count * tp_count
    slot_cap = max(1, 2 * block_rows * top_count // expert_count)
    slot_total = expert_count * slot_cap
    values = whole.astype(jnp.float32)
    center = values - jnp.mean(values, axis=1, keepdims=True)
    spread = jnp.mean(center * center, axis=1, keepdims=True)
    normed = (center * lax.rsqrt(spread + EPSILON) * norm_gain + norm_shift).astype(jnp.bfloat16)
    weights = affinity / jnp.sum(affinity, axis=1, keepdims=True) * ROUTED_SCALE
    contract = (((1,), (1,)), ((), ()))
    shared_g = lax.dot_general(shared_gate, normed, contract, preferred_element_type=jnp.float32)
    shared_u = lax.dot_general(shared_up, normed, contract, preferred_element_type=jnp.float32)
    shared_hidden = (jax.nn.silu(shared_g) * shared_u).astype(jnp.bfloat16)
    own_hidden = lax.all_to_all(shared_hidden, "tp", split_axis=1, concat_axis=0, tiled=True)
    shared_out = lax.dot_general(
        own_hidden, shared_down, (((0,), (0,)), ((), ())), preferred_element_type=jnp.float32
    )
    block_ids = expert_ids.reshape(tp_count, block_rows * top_count)
    ranks = pair_ranks(block_ids, expert_count)
    group_index = block_ids // tp_count
    mine = block_ids % tp_count == tp_index
    block_index = jnp.arange(tp_count, dtype=jnp.int32)[:, None]
    dest = jnp.where(mine, (group_index * tp_count + block_index) * slot_cap + ranks, slot_total)
    token_index = (
        block_index * block_rows
        + jnp.arange(block_rows * top_count, dtype=jnp.int32)[None, :] // top_count
    )
    source_row = (
        jnp.full((slot_total + 1,), tok_count, jnp.int32)
        .at[dest.reshape(-1)]
        .set(token_index.reshape(-1))[:slot_total]
    )
    outgoing = jnp.take(normed, source_row, axis=0, mode="fill", fill_value=0).reshape(
        ep_count, tp_count, slot_cap, width
    )
    incoming = lax.all_to_all(outgoing, "ep", split_axis=0, concat_axis=0, tiled=True)
    result = expert_rows(incoming.reshape(-1, width), expert_gate[0], expert_up[0], expert_down[0])
    returned = lax.all_to_all(
        result.reshape(incoming.shape), "ep", split_axis=0, concat_axis=0, tiled=True
    )
    pair_slot = dest.reshape(tok_count, top_count)
    back_rows = returned.reshape(slot_total, width)
    routed = lax.psum_scatter(
        weighted_sum(back_rows, pair_slot, weights, top_count),
        "tp",
        scatter_dimension=0,
        tiled=True,
    )
    return (routed + shared_out).astype(jnp.bfloat16)


def solution(mesh):
    placed = (
        P("ep", "tp"),
        P(),
        P(),
        P("ep", None),
        P("ep", None),
        P(("ep", "tp"), None, None),
        P(("ep", "tp"), None, None),
        P(("ep", "tp"), None, None),
        P("tp", None),
        P("tp", None),
        P(),
    )
    return jax.shard_map(
        on_device, mesh=mesh, in_specs=placed, out_specs=P(("ep", "tp"), None), check_vma=False
    )
```

profile of v0, /device:TPU:0, one launch (start us, length us, event | category | flops | bytes accessed | tf_op | source)
XLA Modules:
  0.0 271.8 jit_solution(16597467197731617035)
XLA Ops:
  6.5 0.7 all-gather.2.cloned.1.call-update
  7.3 0.9 copy.34
  8.1 0.2 eq.48
  8.3 0.2 reshape.242
  8.5 0.2 eq.52
  8.8 6.9 %reduce-window.6 = s32[8,32,3,128]{3,1,2,0:T(8,128)S(1)} reduce-window(s32[8,32,3,128]{3,1,2,0:T(8,128)S(1)} %fusion.20, s32[]{:T(128)} %constant.82.clone.1), window={size=1x1x1x128 pad=0_0x0_0x0_0x127_0}, to_apply=%region_1.0 | reduce-window | flops 12484608 | bytes 786436 | tf_op jit(solution)/shard_map/reduce-window
  15.8 0.2 slice.78
  15.9 0.2 copy.40
  16.1 0.1 fusion.29
  16.3 0.2 fusion.19
  16.5 0.1 compare_select_fusion
  16.6 11.8 %scatter_custom_fusion = s32[769]{0:T(1024)S(1)} fusion(s32[3072]{0:T(1024)S(1)} %bitcast.82, s32[3072]{0:T(1024)S(1)} %reshape.307, s32[]{:T(128)} %constant.81.clone.1), kind=kCustom, calls=%fused_computation.94 | custom fusion | bytes 3080 | tf_op jit(solution)/shard_map/scatter | solution.py:81
  28.4 0.1 slice.51
  28.5 13.8 %all-gather.2.cloned.1.call-done = bf16[512,2048]{1,0:T(8,128)(2,1)} async-done(((bf16[512,256]{1,0:T(8,128)(2,1)}), bf16[512,2048]{1,0:T(8,128)(2,1)}) %all-gather.2.cloned.1.call-update) | async-done | bytes 2097168 | tf_op jit(solution)/shard_map/all_gather | solution.py:47
  42.3 2.1 convert_reduce_fusion
  44.4 0.1 copy-done.2
  44.5 0.7 fusion.2
  45.2 2.2 fusion.5
  47.4 9.0 %gather_fusion = bf16[768,2048]{1,0:T(8,128)(2,1)} fusion(bf16[512,2048]{1,0:T(8,128)(2,1)} %fusion.5, s32[1024]{0:T(1024)S(1)} %pad_clamp_fusion.6), kind=kCustom, calls=%fused_computation.6 | custom fusion | bytes 6294528 | tf_op jit(solution)/shard_map/jit(_take)/gather | solution.py:83
  56.4 3.9 %broadcast_select_fusion = bf16[4,8,24,2048]{3,2,1,0:T(8,128)(2,1)} fusion(bf16[4,8,24,2048]{3,2,1,0:T(8,128)(2,1)} %bitcast.77, pred[4,8,24]{2,1,0:T(8,128)(4,1)S(1)} %compare_and_fusion), kind=kLoop, calls=%fused_computation.18 | loop fusion | flops 1572864 | bytes 6292224 | tf_op jit(solution)/shard_map/jit(_take)/select_n | solution.py:83
  60.3 4.9 %all-to-all-start = ((bf16[4,8,24,2048]{3,2,1,0:T(8,128)(2,1)}), bf16[4,8,24,2048]{3,2,1,0:T(8,128)(2,1)}, u32[]{:S(2)}, u32[]{:S(2)}) async-start(bf16[4,8,24,2048]{3,2,1,0:T(8,128)(2,1)} %broadcast_select_fusion), calls=%async_computation | async-start | bytes 6291456 | tf_op jit(solution)/shard_map/all_to_all | solution.py:86
  65.2 0.1 add.204
  65.3 0.2 sub.37
  65.5 0.3 fusion.26
  65.8 0.8 slice_reduce_fusion.5
  66.7 35.2 %all-to-all-done = bf16[4,8,24,2048]{3,2,1,0:T(8,128)(2,1)} async-done(((bf16[4,8,24,2048]{3,2,1,0:T(8,128)(2,1)}), bf16[4,8,24,2048]{3,2,1,0:T(8,128)(2,1)}, u32[]{:S(2)}, u32[]{:S(2)}) %all-to-all-start) | async-done | bytes 3145760 | tf_op jit(solution)/shard_map/all_to_all | solution.py:86
  101.9 5.6 %fusion.10 = f32[768,512]{1,0:T(8,128)} fusion(bf16[768,2048]{1,0:T(8,128)(2,1)} %bitcast.5, bf16[1,2048,512]{2,1,0:T(8,128)(2,1)} %param.18), kind=kOutput, calls=%fused_computation.24 | convolution fusion | flops 1610612736 | bytes 6815744 | tf_op jit(solution)/shard_map/dot_general | solution.py:17
  107.4 8.2 %convolution_convert_fusion = bf16[768,2048]{1,0:T(8,128)(2,1)} fusion(bf16[1,512,2048]{2,1,0:T(8,128)(2,1)S(1)} %copy-done, f32[768,512]{1,0:T(8,128)} %fusion.10, bf16[768,2048]{1,0:T(8,128)(2,1)} %bitcast.5, bf16[1,2048,512]{2,1,0:T(8,128)(2,1)} %param.19), kind=kOutput, calls=%fused_computation.17 | convolution fusion | flops 3225157632 | bytes 12058624 | tf_op jit(solution)/shard_map/dot_general | solution.py:20
  115.6 4.6 %all-to-all-start.1 = ((bf16[4,8,24,2048]{3,2,1,0:T(8,128)(2,1)}), bf16[4,8,24,2048]{3,2,1,0:T(8,128)(2,1)}, u32[]{:S(2)}, u32[]{:S(2)}) async-start(bf16[4,8,24,2048]{3,2,1,0:T(8,128)(2,1)} %bitcast.78), calls=%async_computation.1 | async-start | bytes 6291456 | tf_op jit(solution)/shard_map/all_to_all | solution.py:88
  120.5 35.7 %all-to-all-done.1 = bf16[4,8,24,2048]{3,2,1,0:T(8,128)(2,1)} async-done(((bf16[4,8,24,2048]{3,2,1,0:T(8,128)(2,1)}), bf16[4,8,24,2048]{3,2,1,0:T(8,128)(2,1)}, u32[]{:S(2)}, u32[]{:S(2)}) %all-to-all-start.1) | async-done | bytes 3145760 | tf_op jit(solution)/shard_map/all_to_all | solution.py:88
  156.2 7.8 %gather_fusion.6 = bf16[512,2048]{1,0:T(8,128)(2,1)} fusion(bf16[768,2048]{1,0:T(8,128)(2,1)} %bitcast.10, s32[1024]{0:T(1024)S(1)} %pad_clamp_fusion), kind=kCustom, calls=%fused_computation.5.clone | custom fusion | bytes 4196352 | tf_op jit(solution)/shard_map/jit(_take)/gather | solution.py:26
  164.0 7.5 %gather_fusion.5 = bf16[512,2048]{1,0:T(8,128)(2,1)} fusion(bf16[768,2048]{1,0:T(8,128)(2,1)} %bitcast.10, s32[1024]{0:T(1024)S(1)} %pad_clamp_fusion.1), kind=kCustom, calls=%fused_computation.4.clone | custom fusion | bytes 4196352 | tf_op jit(solution)/shard_map/jit(_take)/gather | solution.py:26
  171.6 7.5 %gather_fusion.4 = bf16[512,2048]{1,0:T(8,128)(2,1)} fusion(bf16[768,2048]{1,0:T(8,128)(2,1)} %bitcast.10, s32[1024]{0:T(1024)S(1)} %pad_clamp_fusion.2), kind=kCustom, calls=%fused_computation.3.clone | custom fusion | bytes 4196352 | tf_op jit(solution)/shard_map/jit(_take)/gather | solution.py:26
  179.1 7.5 %gather_fusion.3 = bf16[512,2048]{1,0:T(8,128)(2,1)} fusion(bf16[768,2048]{1,0:T(8,128)(2,1)} %bitcast.10, s32[1024]{0:T(1024)S(1)} %pad_clamp_fusion.3), kind=kCustom, calls=%fused_computation.2.clone | custom fusion | bytes 4196352 | tf_op jit(solution)/shard_map/jit(_take)/gather | solution.py:26
  186.6 7.5 %gather_fusion.2 = bf16[512,2048]{1,0:T(8,128)(2,1)} fusion(bf16[768,2048]{1,0:T(8,128)(2,1)} %bitcast.10, s32[1024]{0:T(1024)S(1)} %pad_clamp_fusion.4), kind=kCustom, calls=%fused_computation.1.clone | custom fusion | bytes 4196352 | tf_op jit(solution)/shard_map/jit(_take)/gather | solution.py:26
  194.1 7.8 %gather_fusion.1 = bf16[512,2048]{1,0:T(8,128)(2,1)} fusion(bf16[768,2048]{1,0:T(8,128)(2,1)} %bitcast.10, s32[1024]{0:T(1024)S(1)} %pad_clamp_fusion.5), kind=kCustom, calls=%fused_computation.clone | custom fusion | bytes 4196352 | tf_op jit(solution)/shard_map/jit(_take)/gather | solution.py:26
  202.0 9.0 %multiply_add_fusion = f32[512,2048]{1,0:T(8,128)} fusion(bf16[512,2048]{1,0:T(8,128)(2,1)} %gather_fusion.6, bf16[512,2048]{1,0:T(8,128)(2,1)} %gather_fusion.5, bf16[512,2048]{1,0:T(8,128)(2,1)} %gather_fusion.4, bf16[512,2048]{1,0:T(8,128)(2,1)} %gather_fusion.3, bf16[512,2048]{1,0:T(8,128)(2,1)} %gather_fusion.2, bf16[512,2048]{1,0:T(8,128)(2,1)} %gather_fusion.1, ...), kind=kLoop, calls=%fused_computation.16 | loop fusion | flops 24117248 | bytes 16792576 | tf_op jit(solution)/shard_map/add | solution.py:27
  211.1 0.9 copy-done.3
  212.0 2.5 convolution_bitcast_fusion.1
  214.5 0.8 fusion.15
  215.3 0.1 copy.46
  215.4 0.2 reshape.338
  215.6 11.3 %all_to_all.29 = bf16[8,2,2048]{2,1,0:T(2,128)(2,1)S(1)} all-to-all(bf16[8,2,2048]{2,1,0:T(2,128)(2,1)S(1)} %reshape.338), channel_id=1, replica_groups=mesh['ep'=4,'tp'=8] {'tp'}, dimensions={0} | all-to-all | bytes 131072 | tf_op jit(solution)/shard_map/all_to_all | solution.py:64
  226.9 0.1 reshape.339
  227.0 0.1 copy.45
  227.1 0.1 all_to_all.25
  227.3 34.9 %reduce-scatter.2.cloned.1.call-done = f32[64,2048]{1,0:T(8,128)} async-done(((f32[512,2048]{1,0:T(8,128)}), f32[64,2048]{1,0:T(8,128)}) %reduce-scatter.2.cloned.1.call-update) | async-done | bytes 524304 | tf_op jit(solution)/shard_map/reduce_scatter | solution.py:93
  262.1 2.9 %fusion.6 = bf16[64,2048]{1,0:T(8,128)(2,1)} fusion(f32[64,2048]{1,0:T(8,128)} %reduce-scatter.2.cloned.1.call-done, bf16[512,64]{0,1:T(8,128)(2,1)S(1)} %all_to_all.25, bf16[512,2048]{1,0:T(8,128)(2,1)} %param.23), kind=kOutput, calls=%fused_computation.20 | convolution fusion | flops 134479872 | bytes 2949120 | tf_op jit(solution)/shard_map/dot_general | solution.py:65
  (50 shorter events, 0.4 us)
Async XLA Ops:
  6.5 100.9 %copy-start = (bf16[1,512,2048]{2,1,0:T(8,128)(2,1)S(1)}, bf16[1,512,2048]{2,1,0:T(8,128)(2,1)}, u32[]{:S(2)}) copy-start(bf16[1,512,2048]{2,1,0:T(8,128)(2,1)} %param.20) | copy-start | bytes 6291460
  6.5 35.8 %all-gather.2.cloned.1.call-start = ((), (), s32[]{:S(2)}) async-start(), calls=%async_computation.4 | async-start | bytes 2359296 | tf_op jit(solution)/shard_map/all_gather | solution.py:47
  42.3 2.2 copy-start.2
  42.3 2.9 %copy-start.5 = (f32[2048]{0:T(1024)S(1)}, f32[2048]{0:T(1024)}, u32[]{:S(2)}) copy-start(f32[2048]{0:T(1024)} %param.15) | copy-start | bytes 24580
  42.3 2.9 %copy-start.6 = (f32[2048]{0:T(1024)S(1)}, f32[2048]{0:T(1024)}, u32[]{:S(2)}) copy-start(f32[2048]{0:T(1024)} %param.14) | copy-start | bytes 24580
  60.3 5.3 %copy-start.4 = (f32[512,6]{0,1:T(8,128)S(1)}, f32[512,6]{0,1:T(8,128)}, u32[]{:S(2)}) copy-start(f32[512,6]{0,1:T(8,128)} %param.17) | copy-start | bytes 36868
  60.3 41.6 %all-to-all-start = ((bf16[4,8,24,2048]{3,2,1,0:T(8,128)(2,1)}), bf16[4,8,24,2048]{3,2,1,0:T(8,128)(2,1)}, u32[]{:S(2)}, u32[]{:S(2)}) async-start(bf16[4,8,24,2048]{3,2,1,0:T(8,128)(2,1)} %broadcast_select_fusion), calls=%async_computation | async-start | bytes 6291456 | tf_op jit(solution)/shard_map/all_to_all | solution.py:86
  115.6 40.6 %all-to-all-start.1 = ((bf16[4,8,24,2048]{3,2,1,0:T(8,128)(2,1)}), bf16[4,8,24,2048]{3,2,1,0:T(8,128)(2,1)}, u32[]{:S(2)}, u32[]{:S(2)}) async-start(bf16[4,8,24,2048]{3,2,1,0:T(8,128)(2,1)} %bitcast.78), calls=%async_computation.1 | async-start | bytes 6291456 | tf_op jit(solution)/shard_map/all_to_all | solution.py:88
  120.3 141.9 %reduce-scatter.2.cloned.1.call-start = ((), (), s32[]{:S(2)}) async-start(), calls=%async_computation.5 | async-start | bytes 4718592 | tf_op jit(solution)/shard_map/reduce_scatter | solution.py:93
  211.0 0.9 copy-start.3
  212.0 2.5 copy-start.1
  212.0 2.5 copy-start.7
Sparse Core Ops, SparseCore 0:
  8.9 33.3 all-gather.1
  211.2 50.8 reduce-scatter.1
where the time goes:
time: 273 us; the launch traced here: 272 us
  waiting for transfers between devices  120 us (44%)
  local copies, waits for them, and re-layouts  71.2 us (26%)
  other arithmetic  25.8 us (9%)
  matrix products  19.9 us (7%)
  between operations  13.8 us (5%)
  blocking collectives  11.3 us (4%)
  starting transfers between devices  9.63 us (4%)
    gather x6, local copies, waits for them, and re-layouts, weighted_sum(): jnp.take(source_rows, slot_index[:, column], axis=0, mode='fill', fill_va...  45.7 us
    all_to_all x1, waiting for transfers between devices, on_device(): lax.all_to_all(result.reshape(incoming.shape), 'ep', split_axis=0, concat...  35.7 us
    all_to_all x1, waiting for transfers between devices, on_device(): lax.all_to_all(outgoing, 'ep', split_axis=0, concat_axis=0, tiled=True)  35.2 us
    reduce_scatter x1, waiting for transfers between devices, on_device(): lax.psum_scatter(weighted_sum(back_rows, pair_slot, weights, top_count),...  34.9 us
    all_gather x1, waiting for transfers between devices, on_device(): whole = lax.all_gather(tokens, 'tp', axis=1, tiled=True)  13.8 us
    scatter x1, local copies, waits for them, and re-layouts, on_device(): source_row = jnp.full((slot_total + 1,), tok_count, jnp.int32).at[dest.re...  11.8 us
    all_to_all x1, blocking collectives, on_device(): lax.all_to_all(shared_hidden, 'tp', split_axis=1, concat_axis=0, tiled=True)  11.3 us
    add x1, other arithmetic, weighted_sum(): total + pair_weight[:, column:column + 1] * picked.astype(jnp.float32)  9.05 us
  transfers between devices with their start and end apart: 4, of which 4 were waited for; matrix products, arithmetic and copies ran while one was open for 10% of the time, Pallas kernels for 0%

commit v1 on v0

--- a/solution.py
+++ b/solution.py
@@ -44,7 +44,8 @@
     ep_count = lax.axis_size("ep")
     tp_count = lax.axis_size("tp")
     tp_index = lax.axis_index("tp")
-    whole = lax.all_gather(tokens, "tp", axis=1, tiled=True)
+    parts = lax.all_gather(tokens, "tp", axis=0, tiled=False)
+    whole = jnp.concatenate(parts, axis=1)
     tok_count = whole.shape[0]
     width = whole.shape[1]
     top_count = expert_ids.shape[1]

time: 273 us -> 272 us (level)
  no operation moved by 1% of the time
where the time goes in v1:
time: 272 us; the launch traced here: 271 us
  waiting for transfers between devices  119 us (44%)
  local copies, waits for them, and re-layouts  71.8 us (26%)
  other arithmetic  27.4 us (10%)
  matrix products  19.9 us (7%)
  between operations  13.8 us (5%)
  blocking collectives  9.86 us (4%)
  starting transfers between devices  9.63 us (4%)
    gather x6, local copies, waits for them, and re-layouts, weighted_sum(): jnp.take(source_rows, slot_index[:, column], axis=0, mode='fill', fill_va...  45.7 us
    all_to_all x1, waiting for transfers between devices, on_device(): lax.all_to_all(result.reshape(incoming.shape), 'ep', split_axis=0, concat...  35.7 us
    all_to_all x1, waiting for transfers between devices, on_device(): lax.all_to_all(outgoing, 'ep', split_axis=0, concat_axis=0, tiled=True)  35.2 us
    reduce_scatter x1, waiting for transfers between devices, on_device(): lax.psum_scatter(weighted_sum(back_rows, pair_slot, weights, top_count),...  34.9 us
    all_gather x1, waiting for transfers between devices, on_device(): parts = lax.all_gather(tokens, 'tp', axis=0, tiled=False)  12.3 us
    scatter x1, local copies, waits for them, and re-layouts, on_device(): source_row = jnp.full((slot_total + 1,), tok_count, jnp.int32).at[dest.re...  11.8 us
    all_to_all x1, blocking collectives, on_device(): lax.all_to_all(shared_hidden, 'tp', split_axis=1, concat_axis=0, tiled=True)  9.86 us
    add x1, other arithmetic, weighted_sum(): total + pair_weight[:, column:column + 1] * picked.astype(jnp.float32)  9.05 us
  transfers between devices with their start and end apart: 4, of which 4 were waited for; matrix products, arithmetic and copies ran while one was open for 10% of the time, Pallas kernels for 0%

profile of v1, /device:TPU:0, one launch (start us, length us, event | category | flops | bytes accessed | tf_op | source)
XLA Modules:
  0.0 271.2 jit_solution(8193581339956051146)
XLA Ops:
  6.5 0.7 all-gather.3.cloned.1.call-update
  7.3 0.9 copy.50
  8.1 0.2 eq.48
  8.3 0.2 reshape.251
  8.5 0.2 eq.52
  8.8 6.9 %reduce-window.6 = s32[8,32,3,128]{3,1,2,0:T(8,128)S(1)} reduce-window(s32[8,32,3,128]{3,1,2,0:T(8,128)S(1)} %fusion.14, s32[]{:T(128)} %constant.82.clone.1), window={size=1x1x1x128 pad=0_0x0_0x0_0x127_0}, to_apply=%region_1.0 | reduce-window | flops 12484608 | bytes 786436 | tf_op jit(solution)/shard_map/reduce-window
  15.8 0.2 slice.78
  15.9 0.2 copy.56
  16.3 0.2 fusion.13
  16.5 0.1 compare_select_fusion
  16.6 11.8 %scatter_custom_fusion = s32[769]{0:T(1024)S(1)} fusion(s32[3072]{0:T(1024)S(1)} %bitcast.91, s32[3072]{0:T(1024)S(1)} %reshape.317, s32[]{:T(128)} %constant.81.clone.1), kind=kCustom, calls=%fused_computation.89 | custom fusion | bytes 3080 | tf_op jit(solution)/shard_map/scatter | solution.py:82
  28.4 0.1 slice.51
  28.5 12.3 %all-gather.3.cloned.1.call-done = bf16[4096,256]{1,0:T(8,128)(2,1)} async-done(((bf16[512,256]{1,0:T(8,128)(2,1)}), bf16[4096,256]{1,0:T(8,128)(2,1)}) %all-gather.3.cloned.1.call-update) | async-done | bytes 2097168 | tf_op jit(solution)/shard_map/all_gather | solution.py:47
  40.8 2.2 convert_reduce_fusion
  43.1 2.3 multiply_reduce_fusion
  45.4 0.6 copy.67
  46.0 0.1 copy-done.4
  46.1 2.1 add_convert_fusion
  48.2 9.0 %gather_fusion = bf16[768,2048]{1,0:T(8,128)(2,1)} fusion(bf16[512,2048]{1,0:T(8,128)(2,1)} %add_convert_fusion, s32[1024]{0:T(1024)S(1)} %pad_clamp_fusion.6), kind=kCustom, calls=%fused_computation.6 | custom fusion | bytes 6294528 | tf_op jit(solution)/shard_map/jit(_take)/gather | solution.py:84
  57.2 3.9 %broadcast_select_fusion = bf16[4,8,24,2048]{3,2,1,0:T(8,128)(2,1)} fusion(bf16[4,8,24,2048]{3,2,1,0:T(8,128)(2,1)} %bitcast.85, pred[4,8,24]{2,1,0:T(8,128)(4,1)S(1)} %compare_and_fusion), kind=kLoop, calls=%fused_computation.12 | loop fusion | flops 1572864 | bytes 6292224 | tf_op jit(solution)/shard_map/jit(_take)/select_n | solution.py:84
  61.1 4.9 %all-to-all-start = ((bf16[4,8,24,2048]{3,2,1,0:T(8,128)(2,1)}), bf16[4,8,24,2048]{3,2,1,0:T(8,128)(2,1)}, u32[]{:S(2)}, u32[]{:S(2)}) async-start(bf16[4,8,24,2048]{3,2,1,0:T(8,128)(2,1)} %broadcast_select_fusion), calls=%async_computation | async-start | bytes 6291456 | tf_op jit(solution)/shard_map/all_to_all | solution.py:87
  66.1 0.1 add.204
  66.1 0.2 sub.45
  66.4 0.3 fusion.20
  66.6 0.8 slice_reduce_fusion.5
  67.5 35.2 %all-to-all-done = bf16[4,8,24,2048]{3,2,1,0:T(8,128)(2,1)} async-done(((bf16[4,8,24,2048]{3,2,1,0:T(8,128)(2,1)}), bf16[4,8,24,2048]{3,2,1,0:T(8,128)(2,1)}, u32[]{:S(2)}, u32[]{:S(2)}) %all-to-all-start) | async-done | bytes 3145760 | tf_op jit(solution)/shard_map/all_to_all | solution.py:87
  102.7 5.6 %fusion.4 = f32[768,512]{1,0:T(8,128)} fusion(bf16[768,2048]{1,0:T(8,128)(2,1)} %bitcast.7, bf16[1,2048,512]{2,1,0:T(8,128)(2,1)} %param.18), kind=kOutput, calls=%fused_computation.18 | convolution fusion | flops 1610612736 | bytes 6815744 | tf_op jit(solution)/shard_map/dot_general | solution.py:17
  108.2 8.2 %convolution_convert_fusion = bf16[768,2048]{1,0:T(8,128)(2,1)} fusion(bf16[1,512,2048]{2,1,0:T(8,128)(2,1)S(1)} %copy-done, f32[768,512]{1,0:T(8,128)} %fusion.4, bf16[768,2048]{1,0:T(8,128)(2,1)} %bitcast.7, bf16[1,2048,512]{2,1,0:T(8,128)(2,1)} %param.19), kind=kOutput, calls=%fused_computation.11 | convolution fusion | flops 3225157632 | bytes 12058624 | tf_op jit(solution)/shard_map/dot_general | solution.py:20
  116.4 4.6 %all-to-all-start.1 = ((bf16[4,8,24,2048]{3,2,1,0:T(8,128)(2,1)}), bf16[4,8,24,2048]{3,2,1,0:T(8,128)(2,1)}, u32[]{:S(2)}, u32[]{:S(2)}) async-start(bf16[4,8,24,2048]{3,2,1,0:T(8,128)(2,1)} %bitcast.87), calls=%async_computation.1 | async-start | bytes 6291456 | tf_op jit(solution)/shard_map/all_to_all | solution.py:89
  121.3 35.7 %all-to-all-done.1 = bf16[4,8,24,2048]{3,2,1,0:T(8,128)(2,1)} async-done(((bf16[4,8,24,2048]{3,2,1,0:T(8,128)(2,1)}), bf16[4,8,24,2048]{3,2,1,0:T(8,128)(2,1)}, u32[]{:S(2)}, u32[]{:S(2)}) %all-to-all-start.1) | async-done | bytes 3145760 | tf_op jit(solution)/shard_map/all_to_all | solution.py:89
  157.0 7.8 %gather_fusion.6 = bf16[512,2048]{1,0:T(8,128)(2,1)} fusion(bf16[768,2048]{1,0:T(8,128)(2,1)} %bitcast.12, s32[1024]{0:T(1024)S(1)} %pad_clamp_fusion), kind=kCustom, calls=%fused_computation.5.clone | custom fusion | bytes 4196352 | tf_op jit(solution)/shard_map/jit(_take)/gather | solution.py:26
  164.8 7.5 %gather_fusion.5 = bf16[512,2048]{1,0:T(8,128)(2,1)} fusion(bf16[768,2048]{1,0:T(8,128)(2,1)} %bitcast.12, s32[1024]{0:T(1024)S(1)} %pad_clamp_fusion.1), kind=kCustom, calls=%fused_computation.4.clone | custom fusion | bytes 4196352 | tf_op jit(solution)/shard_map/jit(_take)/gather | solution.py:26
  172.3 7.5 %gather_fusion.4 = bf16[512,2048]{1,0:T(8,128)(2,1)} fusion(bf16[768,2048]{1,0:T(8,128)(2,1)} %bitcast.12, s32[1024]{0:T(1024)S(1)} %pad_clamp_fusion.2), kind=kCustom, calls=%fused_computation.3.clone | custom fusion | bytes 4196352 | tf_op jit(solution)/shard_map/jit(_take)/gather | solution.py:26
  179.9 7.5 %gather_fusion.3 = bf16[512,2048]{1,0:T(8,128)(2,1)} fusion(bf16[768,2048]{1,0:T(8,128)(2,1)} %bitcast.12, s32[1024]{0:T(1024)S(1)} %pad_clamp_fusion.3), kind=kCustom, calls=%fused_computation.2.clone | custom fusion | bytes 4196352 | tf_op jit(solution)/shard_map/jit(_take)/gather | solution.py:26
  187.4 7.5 %gather_fusion.2 = bf16[512,2048]{1,0:T(8,128)(2,1)} fusion(bf16[768,2048]{1,0:T(8,128)(2,1)} %bitcast.12, s32[1024]{0:T(1024)S(1)} %pad_clamp_fusion.4), kind=kCustom, calls=%fused_computation.1.clone | custom fusion | bytes 4196352 | tf_op jit(solution)/shard_map/jit(_take)/gather | solution.py:26
  194.9 7.8 %gather_fusion.1 = bf16[512,2048]{1,0:T(8,128)(2,1)} fusion(bf16[768,2048]{1,0:T(8,128)(2,1)} %bitcast.12, s32[1024]{0:T(1024)S(1)} %pad_clamp_fusion.5), kind=kCustom, calls=%fused_computation.clone | custom fusion | bytes 4196352 | tf_op jit(solution)/shard_map/jit(_take)/gather | solution.py:26
  202.8 9.0 %multiply_add_fusion = f32[512,2048]{1,0:T(8,128)} fusion(bf16[512,2048]{1,0:T(8,128)(2,1)} %gather_fusion.6, bf16[512,2048]{1,0:T(8,128)(2,1)} %gather_fusion.5, bf16[512,2048]{1,0:T(8,128)(2,1)} %gather_fusion.4, bf16[512,2048]{1,0:T(8,128)(2,1)} %gather_fusion.3, bf16[512,2048]{1,0:T(8,128)(2,1)} %gather_fusion.2, bf16[512,2048]{1,0:T(8,128)(2,1)} %gather_fusion.1, ...), kind=kLoop, calls=%fused_computation.8 | loop fusion | flops 24117248 | bytes 16792576 | tf_op jit(solution)/shard_map/add | solution.py:27
  211.8 0.9 copy-done.2
  212.8 2.5 convolution_bitcast_fusion.1
  215.3 0.8 fusion.9
  216.1 0.1 copy.63
  216.2 0.2 reshape.352
  216.4 9.9 %all_to_all.29 = bf16[8,2,2048]{2,1,0:T(2,128)(2,1)S(1)} all-to-all(bf16[8,2,2048]{2,1,0:T(2,128)(2,1)S(1)} %reshape.352), channel_id=1, replica_groups=mesh['ep'=4,'tp'=8] {'tp'}, dimensions={0} | all-to-all | bytes 131072 | tf_op jit(solution)/shard_map/all_to_all | solution.py:65
  226.2 0.1 reshape.353
  226.4 0.1 copy.62
  226.5 0.1 all_to_all.25
  226.6 34.9 %reduce-scatter.2.cloned.1.call-done = f32[64,2048]{1,0:T(8,128)} async-done(((f32[512,2048]{1,0:T(8,128)}), f32[64,2048]{1,0:T(8,128)}) %reduce-scatter.2.cloned.1.call-update) | async-done | bytes 524304 | tf_op jit(solution)/shard_map/reduce_scatter | solution.py:94
  261.5 2.9 %fusion = bf16[64,2048]{1,0:T(8,128)(2,1)} fusion(f32[64,2048]{1,0:T(8,128)} %reduce-scatter.2.cloned.1.call-done, bf16[512,64]{0,1:T(8,128)(2,1)S(1)} %all_to_all.25, bf16[512,2048]{1,0:T(8,128)(2,1)} %param.23), kind=kOutput, calls=%fused_computation.14 | convolution fusion | flops 134479872 | bytes 2949120 | tf_op jit(solution)/shard_map/dot_general | solution.py:66
  (51 shorter events, 0.5 us)
Async XLA Ops:
  6.5 101.7 %copy-start = (bf16[1,512,2048]{2,1,0:T(8,128)(2,1)S(1)}, bf16[1,512,2048]{2,1,0:T(8,128)(2,1)}, u32[]{:S(2)}) copy-start(bf16[1,512,2048]{2,1,0:T(8,128)(2,1)} %param.20) | copy-start | bytes 6291460
  6.5 34.3 %all-gather.3.cloned.1.call-start = ((), (), s32[]{:S(2)}) async-start(), calls=%async_computation.5 | async-start | bytes 2359296 | tf_op jit(solution)/shard_map/all_gather | solution.py:47
  45.4 0.7 copy-start.4
  45.4 0.7 copy-start.5
  61.1 5.0 %copy-start.3 = (f32[512,6]{0,1:T(8,128)S(1)}, f32[512,6]{0,1:T(8,128)}, u32[]{:S(2)}) copy-start(f32[512,6]{0,1:T(8,128)} %param.17) | copy-start | bytes 36868
  61.1 41.6 %all-to-all-start = ((bf16[4,8,24,2048]{3,2,1,0:T(8,128)(2,1)}), bf16[4,8,24,2048]{3,2,1,0:T(8,128)(2,1)}, u32[]{:S(2)}, u32[]{:S(2)}) async-start(bf16[4,8,24,2048]{3,2,1,0:T(8,128)(2,1)} %broadcast_select_fusion), calls=%async_computation | async-start | bytes 6291456 | tf_op jit(solution)/shard_map/all_to_all | solution.py:87
  116.4 40.6 %all-to-all-start.1 = ((bf16[4,8,24,2048]{3,2,1,0:T(8,128)(2,1)}), bf16[4,8,24,2048]{3,2,1,0:T(8,128)(2,1)}, u32[]{:S(2)}, u32[]{:S(2)}) async-start(bf16[4,8,24,2048]{3,2,1,0:T(8,128)(2,1)} %bitcast.87), calls=%async_computation.1 | async-start | bytes 6291456 | tf_op jit(solution)/shard_map/all_to_all | solution.py:89
  121.1 140.4 %reduce-scatter.2.cloned.1.call-start = ((), (), s32[]{:S(2)}) async-start(), calls=%async_computation.4 | async-start | bytes 4718592 | tf_op jit(solution)/shard_map/reduce_scatter | solution.py:94
  211.8 0.9 copy-start.2
  212.8 2.5 copy-start.1
  212.8 2.5 copy-start.6
Sparse Core Ops, SparseCore 0:
  8.9 31.8 all-gather.2
  212.0 49.4 reduce-scatter.1
